TPU v7x, 32 devices: a whole 2x2x4 slice. The times are simulated.
32 devices in a mesh: grp: 2 (over x), kv: 4 (over z), tp: 4 (over y, core).
Axes of the slice: x: 2, y: 2, z: 4, core: 2. Of those that a mesh axis runs over, the one named last changes fastest.
Arguments:
- stream: bfloat16 [32, 4096], P('grp', ('kv', 'tp')), parts along dimension 0, may hold values from -6 to 6
- attn_gain: bfloat16 [4096], P('kv'), may hold values from 0.099609375 to 1.8984375
- mlp_gain: bfloat16 [4096], P('kv'), may hold values from 0.099609375 to 1.8984375
- w_query: bfloat16 [4096, 4096], P('kv', 'tp'), may hold values from -0.09375 to 0.09375
- w_key: bfloat16 [4096, 4096], P('kv', 'tp'), may hold values from -0.09375 to 0.09375
- w_value: bfloat16 [4096, 4096], P('kv', 'tp'), may hold values from -0.09375 to 0.09375
- w_zgate: bfloat16 [4096, 4096], P('kv', 'tp'), may hold values from -0.09375 to 0.09375
- w_decay: bfloat16 [4096, 32], P('kv'), may hold values from -0.09375 to 0.09375
- w_beta: bfloat16 [4096, 32], P('kv'), may hold values from -0.09375 to 0.09375
- decay_rate: float32 [32], P('tp'), may hold values from 0.03 to 3
- head_gain: float32 [128], replicated, may hold values from 0.1 to 1.9
- w_attn_out: bfloat16 [4096, 4096], P('tp', 'kv'), may hold values from -0.09375 to 0.09375
- w_gate: bfloat16 [4096, 11264], P('kv', 'tp'), may hold values from -0.09375 to 0.09375
- w_up: bfloat16 [4096, 11264], P('kv', 'tp'), may hold values from -0.09375 to 0.09375
- w_down: bfloat16 [11264, 4096], P('tp', 'kv'), may hold values from -0.0546875 to 0.0546875
- state: float32 [32, 32, 128, 128], P(('grp', 'kv'), 'tp'), parts along dimension 0, may hold values from -4 to 4
Outputs:
- next_stream: bfloat16 [32, 4096], P('grp', ('kv', 'tp')), parts along dimension 0
- new_state: float32 [32, 32, 128, 128], P(('grp', 'kv'), 'tp'), parts along dimension 0
There are 2 independent parts, one for each index of `grp`. A program takes and returns all parts, laid end to end along the dimension named above; an argument that names none is the same for every part. Nothing has to cross between parts.
All inputs are finite; a program needn't handle non-finite values.
Results may differ from a plain program's by a relative error of at most 0.025.
Values may be sent and summed in bfloat16 or wider, within the bound.
No kernel may reach another device: no remote copies, remote signals or barrier semaphores. Data moves between devices by JAX's collectives and lax.ppermute only.
A program may use at most 64 MiB of HBM per device.

v0:
```python
import jax
import jax.numpy as jnp
from jax import lax
from jax.sharding import PartitionSpec as P

D = 4096
HEAD_DIM = 128
EPSILON = 1e-06


def l2_unit(values):
    return values * lax.rsqrt(jnp.sum(values * values, axis=-1, keepdims=True) + EPSILON)


def delta_update(query, key_vec, value_vec, log_decay, beta_gate, state):
    decayed = jnp.exp(log_decay)[..., None, None] * state
    recalled = jnp.einsum("shkv,shk->shv", decayed, key_vec, precision=lax.Precision.HIGHEST)
    update = beta_gate[..., None] * (value_vec - recalled)
    new_state = decayed + key_vec[..., :, None] * update[..., None, :]
    head_out = jnp.einsum("shkv,shk->shv", new_state, query, precision=lax.Precision.HIGHEST)
    return (new_state, head_out)


def head_mix(head_out, head_gain, z_gate):
    scaled = head_out * lax.rsqrt(jnp.mean(head_out * head_out, axis=-1, keepdims=True) + EPSILON)
    return (scaled * head_gain * jax.nn.silu(z_gate)).astype(jnp.bfloat16)


def local(
    stream,
    attn_gain,
    mlp_gain,
    w_query,
    w_key,
    w_value,
    w_zgate,
    w_decay,
    w_beta,
    decay_rate,
    head_gain,
    w_attn_out,
    w_gate,
    w_up,
    w_down,
    state,
):
    seq_count = state.shape[0]
    local_heads = state.shape[1]
    width = w_query.shape[1]
    heads_total = w_decay.shape[1]
    kv_offset = lax.axis_index("kv") * seq_count
    head_offset = lax.axis_index("tp") * local_heads
    block_rows = lax.all_gather(stream, "tp", axis=1, tiled=True).astype(jnp.float32)
    local_squares = jnp.sum(block_rows * block_rows, axis=1)
    normed = (block_rows * attn_gain.astype(jnp.float32)[None, :]).astype(jnp.bfloat16)
    small_weights = jnp.concatenate([w_decay, w_beta], axis=1)
    pieces = [
        jnp.dot(normed, weight, preferred_element_type=jnp.float32)
        for weight in (w_query, w_key, w_value, w_zgate)
    ]
    small = jnp.dot(normed, small_weights, preferred_element_type=jnp.float32)
    own_decay = lax.dynamic_slice_in_dim(small, head_offset, local_heads, 1)
    own_beta = lax.dynamic_slice_in_dim(small, heads_total + head_offset, local_heads, 1)
    summed = lax.psum_scatter(
        jnp.concatenate(pieces + [own_decay, own_beta], axis=1).astype(jnp.bfloat16),
        "kv",
        scatter_dimension=0,
        tiled=True,
    ).astype(jnp.float32)
    total_squares = lax.psum(local_squares, "kv")
    row_scale = lax.rsqrt(total_squares / D + EPSILON)
    own_scale = lax.dynamic_slice_in_dim(row_scale, kv_offset, seq_count, 0)
    summed = summed * own_scale[:, None]

    def head_block(index):
        return summed[:, index * width : (index + 1) * width].reshape(
            seq_count, local_heads, HEAD_DIM
        )

    query = l2_unit(head_block(0)) * HEAD_DIM ** (-0.5)
    key_vec = l2_unit(head_block(1))
    value_vec = head_block(2)
    z_gate = head_block(3)
    log_decay = -decay_rate[None, :] * jax.nn.softplus(
        summed[:, 4 * width : 4 * width + local_heads]
    )
    beta_gate = jax.nn.sigmoid(summed[:, 4 * width + local_heads :])
    new_state, head_out = delta_update(query, key_vec, value_vec, log_decay, beta_gate, state)
    mixed = head_mix(head_out, head_gain, z_gate).reshape(seq_count, width)
    attn_part = jnp.dot(
        lax.all_gather(mixed, "kv", axis=0, tiled=True),
        w_attn_out,
        preferred_element_type=jnp.float32,
    )
    attn_sum = lax.psum_scatter(
        attn_part.astype(jnp.bfloat16), "tp", scatter_dimension=1, tiled=True
    ).astype(jnp.float32)
    residual_stream = (stream.astype(jnp.float32) + attn_sum).astype(jnp.bfloat16)
    mlp_block = lax.all_gather(residual_stream, "tp", axis=1, tiled=True).astype(jnp.float32)
    mlp_local_squares = jnp.sum(mlp_block * mlp_block, axis=1)
    mlp_total_squares = lax.psum(mlp_local_squares, "kv")
    normed_mlp = (mlp_block * mlp_gain.astype(jnp.float32)[None, :]).astype(jnp.bfloat16)
    gate_part = jnp.dot(normed_mlp, w_gate, preferred_element_type=jnp.float32)
    up_part = jnp.dot(normed_mlp, w_up, preferred_element_type=jnp.float32)
    operands = (gate_part, up_part)
    totals = (
        lax.psum(operands[0].astype(jnp.bfloat16), "kv").astype(jnp.float32),
        lax.psum(operands[1].astype(jnp.bfloat16), "kv").astype(jnp.float32),
    )
    gate_sum, up_sum = (totals[0], totals[1])
    mlp_scale = lax.rsqrt(mlp_total_squares / D + EPSILON)
    hidden = (jax.nn.silu(gate_sum * mlp_scale[:, None]) * (up_sum * mlp_scale[:, None])).astype(
        jnp.bfloat16
    )
    down_part = jnp.dot(hidden, w_down, preferred_element_type=jnp.float32)
    mlp_sum = lax.psum_scatter(
        down_part.astype(jnp.bfloat16), "tp", scatter_dimension=1, tiled=True
    ).astype(jnp.float32)
    next_stream = (residual_stream.astype(jnp.float32) + mlp_sum).astype(jnp.bfloat16)
    return (next_stream, new_state)


def solution(mesh):
    return jax.shard_map(
        local,
        mesh=mesh,
        in_specs=(
            P("grp", ("kv", "tp")),
            P("kv"),
            P("kv"),
            P("kv", "tp"),
            P("kv", "tp"),
            P("kv", "tp"),
            P("kv", "tp"),
            P("kv", None),
            P("kv", None),
            P("tp"),
            P(),
            P("tp", "kv"),
            P("kv", "tp"),
            P("kv", "tp"),
            P("tp", "kv"),
            P(("grp", "kv"), "tp", None, None),
        ),
        out_specs=(P("grp", ("kv", "tp")), P(("grp", "kv"), "tp", None, None)),
        check_vma=False,
    )
```

profile of v0, /device:TPU:0, one launch (start us, length us, event | category | flops | bytes accessed | tf_op | source)
XLA Modules:
  0.0 189.6 jit_solution(2436157586402226002)
XLA Ops:
  7.2 0.0 copy-start
  7.2 0.0 all-reduce.5.cloned.1.call-start
  7.2 0.0 copy-start.3
  7.2 0.8 convert_element_type.66
  8.1 6.6 %all_gather.9 = bf16[16,1024]{1,0:T(8,128)(2,1)S(1)} all-gather(bf16[16,256]{1,0:T(8,128)(2,1)} %param.16), channel_id=1, replica_groups=mesh['grp'=2,'kv'=4,'tp'=4] {'tp'}, dimensions={1}, use_global_device_ids=true | all-gather | bytes 40960 | tf_op jit(solution)/shard_map/all_gather | solution.py:53
  14.7 0.0 copy-done
  14.7 0.0 copy-start.4
  14.7 0.4 convolution_convert_fusion.6
  15.1 0.0 copy-done.3
  15.1 0.4 convolution_convert_fusion.5
  15.5 0.8 copy-done.4
  16.3 0.4 convolution_convert_fusion.4
  16.7 0.3 copy-done.5
  17.0 0.4 convolution_convert_fusion.7
  17.4 0.0 copy-done.9
  17.4 0.0 copy-done.10
  17.4 0.1 fusion.3
  17.5 0.1 dynamic-slice_convert_fusion
  17.6 0.8 concatenate.8
  18.4 0.0 all-reduce.5.cloned.1.call-update
  18.4 0.0 reduce-scatter.3.cloned.1.call-start
  18.5 0.1 fusion.10
  18.6 0.0 copy-done.11
  18.6 12.4 %psum.28 = f32[16]{0:T(128)S(1)} all-reduce(f32[16]{0:T(128)S(1)} %fusion.10), channel_id=1, replica_groups=mesh['grp'=2,'kv'=4,'tp'=4] {'kv'}, use_global_device_ids=true, to_apply=%region_2.0 | all-reduce | flops 16 | bytes 128 | tf_op jit(solution)/shard_map/psum | solution.py:70
  31.0 0.0 copy-done.12
  31.0 0.6 dynamic-slice
  32.3 0.1 dynamic_slice.11
  32.3 22.4 %all-reduce.5.cloned.1.call-done = bf16[16,4112]{1,0:T(8,128)(2,1)} async-done(((bf16[16,4112]{1,0:T(8,128)(2,1)}), bf16[16,4112]{1,0:T(8,128)(2,1)}) %all-reduce.5.cloned.1.call-update) | async-done | bytes 131600
  54.8 1.1 convert_multiply_fusion.4
  55.9 0.1 fusion.33
  56.0 0.1 fusion.22
  56.1 0.1 bitcast_multiply_fusion.3
  56.2 3.6 %fusion = f32[4,8,1,128]{3,2,1,0:T(1,128)S(1)} fusion(f32[4,8,128,1]{2,3,1,0:T(1,128)S(1)} %bitcast.62, f32[4,8,128,128]{3,2,1,0:T(8,128)} %param.31, f32[4,8]{1,0:T(4,128)S(1)} %get-tuple-element.9), kind=kOutput, calls=%fused_computation.3 | convolution fusion | flops 6815744 | bytes 2130048 | tf_op jit(solution)/shard_map/shkv,shk->shv/dot_general | solution.py:17
  59.8 0.1 fusion.19
  59.9 0.1 fusion.20
  59.9 0.0 copy-done.1
  59.9 0.7 multiply_add_fusion
  60.7 0.0 copy-start.2
  60.7 0.0 copy-start.8
  60.7 1.3 copy-done.2
  62.0 1.9 fusion.36
  63.9 0.1 multiply_reduce_fusion
  64.0 0.0 copy-done.8
  64.0 0.1 fusion.23
  64.1 13.1 %all-gather = bf16[4,4,1024]{2,1,0:T(4,128)(2,1)S(1)} all-gather(bf16[1,4,1024]{2,1,0:T(4,128)(2,1)S(1)} %reshape.59), channel_id=1, replica_groups=mesh['grp'=2,'kv'=4,'tp'=4] {'kv'}, dimensions={0}, use_global_device_ids=true | all-gather | bytes 40960 | tf_op jit(solution)/shard_map/all_gather | solution.py:91
  77.3 2.6 %convolution_convert_fusion.3 = bf16[16,1024]{1,0:T(8,128)(2,1)} fusion(bf16[16,1024]{1,0:T(8,128)(2,1)S(1)} %reshape.60, bf16[1024,1024]{1,0:T(8,128)(2,1)} %param.27), kind=kOutput, calls=%fused_computation.6 | convolution fusion | flops 33570816 | bytes 2162688 | tf_op jit(solution)/shard_map/dot_general | solution.py:90
  79.8 0.0 reduce-scatter.3.cloned.1.call-update
  79.9 0.0 all-reduce.7.cloned.1.call-start
  79.9 0.0 copy-done.7
  79.9 19.6 %reduce-scatter.3.cloned.1.call-done = bf16[16,256]{1,0:T(8,128)(2,1)} async-done(((bf16[16,1024]{1,0:T(8,128)(2,1)}), bf16[16,256]{1,0:T(8,128)(2,1)}) %reduce-scatter.3.cloned.1.call-update) | async-done | bytes 8208 | tf_op jit(solution)/shard_map/reduce_scatter | solution.py:95
  99.6 0.0 copy-done.6
  99.6 0.7 add_convert_fusion.1
  100.3 5.2 %all_gather.11 = bf16[16,1024]{1,0:T(8,128)(2,1)S(1)} all-gather(bf16[16,256]{1,0:T(8,128)(2,1)S(1)} %add_convert_fusion.1), channel_id=1, replica_groups=mesh['grp'=2,'kv'=4,'tp'=4] {'tp'}, dimensions={1}, use_global_device_ids=true | all-gather | bytes 40960 | tf_op jit(solution)/shard_map/all_gather | solution.py:99
  105.5 0.1 fusion.12
  105.6 11.7 %psum.30 = f32[16]{0:T(128)S(1)} all-reduce(f32[16]{0:T(128)S(1)} %fusion.12), channel_id=1, replica_groups=mesh['grp'=2,'kv'=4,'tp'=4] {'kv'}, use_global_device_ids=true, to_apply=%region_9.10 | all-reduce | flops 16 | bytes 128 | tf_op jit(solution)/shard_map/psum | solution.py:101
  117.3 4.1 %convolution_convert_fusion = bf16[16,2816]{1,0:T(8,128)(2,1)} fusion(bf16[1024,2816]{1,0:T(8,128)(2,1)} %param.29, bf16[16,1024]{1,0:T(8,128)(2,1)S(1)} %all_gather.11, f32[1024]{0:T(1024)S(1)} %convert_element_type.75), kind=kOutput, calls=%fused_computation | convolution fusion | flops 92368896 | bytes 5894144 | tf_op jit(solution)/shard_map/dot_general | solution.py:104
  121.4 4.1 %convolution_convert_fusion.1 = bf16[16,2816]{1,0:T(8,128)(2,1)} fusion(bf16[1024,2816]{1,0:T(8,128)(2,1)} %param.28, bf16[16,1024]{1,0:T(8,128)(2,1)S(1)} %all_gather.11, f32[1024]{0:T(1024)S(1)} %convert_element_type.75), kind=kOutput, calls=%fused_computation.1 | convolution fusion | flops 92368896 | bytes 5894144 | tf_op jit(solution)/shard_map/dot_general | solution.py:103
  125.6 0.0 all-reduce.7.cloned.1.call-update
  125.6 0.0 reduce-scatter.5.cloned.1.call-start
  125.7 32.1 %all-reduce.7.cloned.1.call-done = (bf16[16,2816]{1,0:T(8,128)(2,1)}, bf16[16,2816]{1,0:T(8,128)(2,1)}) async-done(((bf16[16,2816]{1,0:T(8,128)(2,1)}, bf16[16,2816]{1,0:T(8,128)(2,1)}), (bf16[16,2816]{1,0:T(8,128)(2,1)}, bf16[16,2816]{1,0:T(8,128)(2,1)})) %all-reduce.7.cloned.1.call-update) | async-done | bytes 180240 | tf_op jit(solution)/shard_map/psum | solution.py:108
  157.7 4.3 %convolution_convert_fusion.2 = bf16[16,1024]{1,0:T(8,128)(2,1)} fusion(bf16[2816,1024]{1,0:T(8,128)(2,1)} %param.30, bf16[16,2816]{1,0:T(8,128)(2,1)} %get-tuple-element.2, bf16[16,2816]{1,0:T(8,128)(2,1)} %get-tuple-element.3, f32[16]{0:T(128)S(1)} %add_rsqrt_fusion.3), kind=kOutput, calls=%fused_computation.5 | convolution fusion | flops 92741632 | bytes 5980224 | tf_op jit(solution)/shard_map/dot_general | solution.py:115
  162.0 0.0 reduce-scatter.5.cloned.1.call-update
  162.0 19.8 %reduce-scatter.5.cloned.1.call-done = bf16[16,256]{1,0:T(8,128)(2,1)} async-done(((bf16[16,1024]{1,0:T(8,128)(2,1)}), bf16[16,256]{1,0:T(8,128)(2,1)}) %reduce-scatter.5.cloned.1.call-update) | async-done | bytes 8208 | tf_op jit(solution)/shard_map/reduce_scatter | solution.py:116
  181.8 1.3 add_convert_fusion
  (18 shorter events, 0.1 us)
Async XLA Ops:
  7.2 7.5 %copy-start = (bf16[1024,1024]{1,0:T(8,128)(2,1)S(1)}, bf16[1024,1024]{1,0:T(8,128)(2,1)}, u32[]{:S(2)}) copy-start(bf16[1024,1024]{1,0:T(8,128)(2,1)} %param.20) | copy-start | bytes 6291460
  7.2 47.6 %all-reduce.5.cloned.1.call-start = ((), (), s32[]{:S(2)}) async-start(), calls=%async_computation.4 | async-start | bytes 270336
  7.2 7.8 %copy-start.3 = (bf16[1024,1024]{1,0:T(8,128)(2,1)S(1)}, bf16[1024,1024]{1,0:T(8,128)(2,1)}, u32[]{:S(2)}) copy-start(bf16[1024,1024]{1,0:T(8,128)(2,1)} %param.21) | copy-start | bytes 6291460
  14.7 1.6 copy-start.4
  15.1 1.9 %copy-start.5 = (bf16[1024,1024]{1,0:T(8,128)(2,1)S(1)}, bf16[1024,1024]{1,0:T(8,128)(2,1)}, u32[]{:S(2)}) copy-start(bf16[1024,1024]{1,0:T(8,128)(2,1)} %param.19) | copy-start | bytes 6291460
  16.3 1.1 copy-start.9
  16.3 1.1 copy-start.10
  16.3 2.3 %copy-start.11 = (f32[8]{0:T(128)S(1)}, f32[8]{0:T(128)}, u32[]{:S(2)}) copy-start(f32[8]{0:T(128)} %param.25) | copy-start | bytes 100
  16.3 14.7 %copy-start.12 = (u32[32]{0:T(128)S(1)}, u32[32]{0:T(128)}, u32[]{:S(2)}) copy-start(u32[32]{0:T(128)} %constant.46) | copy-start | bytes 388
  18.4 81.2 %reduce-scatter.3.cloned.1.call-start = ((), (), s32[]{:S(2)}) async-start(), calls=%async_computation.2 | async-start | bytes 40960 | tf_op jit(solution)/shard_map/reduce_scatter | solution.py:95
  54.8 5.2 %copy-start.1 = (f32[4,8,128,128]{3,2,1,0:T(8,128)S(1)}, f32[4,8,128,128]{3,2,1,0:T(8,128)}, u32[]{:S(2)}) copy-start(f32[4,8,128,128]{3,2,1,0:T(8,128)} %param.31) | copy-start | bytes 6291460
  60.7 1.3 copy-start.2
  60.7 3.3 %copy-start.8 = (f32[128]{0:T(128)S(1)}, f32[128]{0:T(128)}, u32[]{:S(2)}) copy-start(f32[128]{0:T(128)} %param.26) | copy-start | bytes 1540
  62.0 17.9 %copy-start.7 = (bf16[1024]{0:T(1024)(128)(2,1)S(1)}, bf16[1024]{0:T(1024)(128)(2,1)}, u32[]{:S(2)}) copy-start(bf16[1024]{0:T(1024)(128)(2,1)} %param.18) | copy-start | bytes 6148
  62.0 37.6 %copy-start.6 = (bf16[16,256]{1,0:T(8,128)(2,1)S(1)}, bf16[16,256]{1,0:T(8,128)(2,1)}, u32[]{:S(2)}) copy-start(bf16[16,256]{1,0:T(8,128)(2,1)} %param.16) | copy-start | bytes 24580
  79.9 77.9 %all-reduce.7.cloned.1.call-start = ((), (), s32[]{:S(2)}) async-start(), calls=%async_computation.5 | async-start | bytes 360448 | tf_op jit(solution)/shard_map/psum | solution.py:108
  125.6 56.2 %reduce-scatter.5.cloned.1.call-start = ((), (), s32[]{:S(2)}) async-start(), calls=%async_computation.3 | async-start | bytes 40960 | tf_op jit(solution)/shard_map/reduce_scatter | solution.py:116
Sparse Core Ops, SparseCore 0:
  18.5 36.2 all-reduce.4
  80.0 19.5 reduce-scatter.2
  125.7 31.9 all-reduce.6
  162.1 19.5 reduce-scatter.4
where the time goes:
time: 190 us
  waiting for transfers between devices  94 us (49%)
  blocking collectives  49 us (26%)
  matrix products  22.3 us (12%)
  between operations  14.6 us (8%)
  other arithmetic  5.53 us (3%)
  local copies, waits for them, and re-layouts  4.03 us (2%)
    psum x1, waiting for transfers between devices, local(): lax.psum(operands[1].astype(jnp.bfloat16), 'kv').astype(jnp.float32)  32.1 us
    unnamed x5, waiting for transfers between devices  22.5 us
    reduce_scatter x1, waiting for transfers between devices, local(): lax.psum_scatter(down_part.astype(jnp.bfloat16), 'tp', scatter_dimension=...  19.8 us
    reduce_scatter x1, waiting for transfers between devices, local(): lax.psum_scatter(attn_part.astype(jnp.bfloat16), 'tp', scatter_dimension=...  19.6 us
    all_gather x1, blocking collectives, local(): lax.all_gather(mixed, 'kv', axis=0, tiled=True)  13.1 us
    psum x1, blocking collectives, local(): total_squares = lax.psum(local_squares, 'kv')  12.4 us
    psum x1, blocking collectives, local(): mlp_total_squares = lax.psum(mlp_local_squares, 'kv')  11.7 us
    all_gather x1, blocking collectives, local(): lax.all_gather(stream, 'tp', axis=1, tiled=True).astype(jnp.float32)  6.6 us
  transfers between devices with their start and end apart: 4, of which 4 were waited for; matrix products, arithmetic and copies ran while one was open for 0% of the time, Pallas kernels for 0%

commit v1 on v0

--- a/solution.py
+++ b/solution.py
@@ -105,7 +105,7 @@
     operands = (gate_part, up_part)
     totals = (
         lax.psum(operands[0].astype(jnp.bfloat16), "kv").astype(jnp.float32),
-        lax.psum(operands[1].astype(jnp.bfloat16), "kv").astype(jnp.float32),
+        jnp.sum(lax.all_gather(operands[1].astype(jnp.bfloat16), "kv"), axis=0).astype(jnp.float32),
     )
     gate_sum, up_sum = (totals[0], totals[1])
     mlp_scale = lax.rsqrt(mlp_total_squares / D + EPSILON)

time: 190 us -> 180 us (0.947)
  waiting for transfers between devices: 94 us -> 70.5 us
  blocking collectives: 49 us -> 63.2 us
    psum x1, waiting for transfers between devices: 32.1 us -> 8.59 us  [local(): lax.psum(operands[0].astype(jnp.bfloat16), 'kv').astype(jnp.float32)]
    all_gather x0 -> x1, blocking collectives: none -> 14.1 us  [local(): lax.all_gather(operands[1].astype(jnp.bfloat16), 'kv')]
where the time goes in v1:
time: 180 us; the launch traced here: 179 us
  waiting for transfers between devices  70.5 us (39%)
  blocking collectives  63.2 us (35%)
  matrix products  21.6 us (12%)
  between operations  14.6 us (8%)
  other arithmetic  5.43 us (3%)
  local copies, waits for them, and re-layouts  3.95 us (2%)
    unnamed x5, waiting for transfers between devices  22.5 us
    reduce_scatter x1, waiting for transfers between devices, local(): lax.psum_scatter(down_part.astype(jnp.bfloat16), 'tp', scatter_dimension=...  19.7 us
    reduce_scatter x1, waiting for transfers between devices, local(): lax.psum_scatter(attn_part.astype(jnp.bfloat16), 'tp', scatter_dimension=...  19.6 us
    all_gather x1, blocking collectives, local(): lax.all_gather(operands[1].astype(jnp.bfloat16), 'kv')  14.1 us
    all_gather x1, blocking collectives, local(): lax.all_gather(mixed, 'kv', axis=0, tiled=True)  13.1 us
    psum x1, blocking collectives, local(): total_squares = lax.psum(local_squares, 'kv')  12.4 us
    psum x1, blocking collectives, local(): mlp_total_squares = lax.psum(mlp_local_squares, 'kv')  11.8 us
    psum x1, waiting for transfers between devices, local(): lax.psum(operands[0].astype(jnp.bfloat16), 'kv').astype(jnp.float32)  8.59 us
  transfers between devices with their start and end apart: 4, of which 4 were waited for; matrix products, arithmetic and copies ran while one was open for 0% of the time, Pallas kernels for 0%

profile of v1, /device:TPU:0, one launch (start us, length us, event | category | flops | bytes accessed | tf_op | source)
XLA Modules:
  0.0 179.4 jit_solution(9377656124833021262)
XLA Ops:
  7.2 0.0 copy-start
  7.2 0.0 all-reduce.6.cloned.1.call-start
  7.2 0.0 copy-start.3
  7.2 6.6 %all_gather.15 = bf16[16,1024]{1,0:T(8,128)(2,1)S(1)} all-gather(bf16[16,256]{1,0:T(8,128)(2,1)} %param.16), channel_id=1, replica_groups=mesh['grp'=2,'kv'=4,'tp'=4] {'tp'}, dimensions={1}, use_global_device_ids=true | all-gather | bytes 40960 | tf_op jit(solution)/shard_map/all_gather | solution.py:53
  13.9 0.7 convert_element_type.68
  14.5 0.0 copy-done
  14.5 0.4 convolution_convert_fusion.4
  14.9 0.0 copy-done.3
  14.9 0.4 convolution_convert_fusion.5
  15.3 0.8 copy-done.4
  16.1 0.4 convolution_convert_fusion.6
  16.5 0.3 copy-done.5
  16.9 0.4 convolution_convert_fusion.7
  17.3 0.0 copy-done.9
  17.3 0.0 copy-done.10
  17.3 0.1 fusion.3
  17.4 0.1 dynamic-slice_convert_fusion
  17.5 0.8 concatenate.8
  18.2 0.0 all-reduce.6.cloned.1.call-update
  18.3 0.0 reduce-scatter.3.cloned.1.call-start
  18.3 0.1 fusion.10
  18.4 12.4 %psum.21 = f32[16]{0:T(128)S(1)} all-reduce(f32[16]{0:T(128)S(1)} %fusion.10), channel_id=1, replica_groups=mesh['grp'=2,'kv'=4,'tp'=4] {'kv'}, use_global_device_ids=true, to_apply=%region_2.0 | all-reduce | flops 16 | bytes 128 | tf_op jit(solution)/shard_map/psum | solution.py:70
  30.8 0.0 copy-done.11
  30.9 0.1 dynamic_slice.11
  30.9 0.0 copy-done.12
  30.9 0.6 dynamic-slice
  32.2 22.5 %all-reduce.6.cloned.1.call-done = bf16[16,4112]{1,0:T(8,128)(2,1)} async-done(((bf16[16,4112]{1,0:T(8,128)(2,1)}), bf16[16,4112]{1,0:T(8,128)(2,1)}) %all-reduce.6.cloned.1.call-update) | async-done | bytes 131600
  54.7 1.1 convert_multiply_fusion.4
  55.8 0.1 fusion.22
  55.9 0.1 bitcast_multiply_fusion.3
  56.0 0.1 fusion.33
  56.0 3.6 %fusion = f32[4,8,1,128]{3,2,1,0:T(1,128)S(1)} fusion(f32[4,8,128,1]{2,3,1,0:T(1,128)S(1)} %bitcast.64, f32[4,8,128,128]{3,2,1,0:T(8,128)} %param.31, f32[4,8]{1,0:T(4,128)S(1)} %get-tuple-element.7), kind=kOutput, calls=%fused_computation.3 | convolution fusion | flops 6815744 | bytes 2130048 | tf_op jit(solution)/shard_map/shkv,shk->shv/dot_general | solution.py:17
  59.6 0.1 fusion.19
  59.7 0.0 copy-done.1
  59.7 0.8 multiply_add_fusion
  60.5 0.0 copy-start.2
  60.5 0.0 copy-start.8
  60.5 0.1 fusion.20
  60.6 1.2 copy-done.2
  61.8 1.9 %fusion.36 = f32[4,8,1,128]{3,2,1,0:T(1,128)S(1)} fusion(f32[4,8,128,128]{3,2,1,0:T(8,128)S(1)} %multiply_add_fusion, f32[4,8,128,1]{2,3,1,0:T(1,128)S(1)} %bitcast.68), kind=kOutput, calls=%fused_computation.67 | convolution fusion | flops 6291456 | bytes 2129920 | tf_op jit(solution)/shard_map/shkv,shk->shv/dot_general | solution.py:20
  63.7 0.1 multiply_reduce_fusion
  63.8 0.0 copy-done.8
  63.8 0.1 fusion.23
  63.9 13.1 %all-gather.1 = bf16[4,4,1024]{2,1,0:T(4,128)(2,1)S(1)} all-gather(bf16[1,4,1024]{2,1,0:T(4,128)(2,1)S(1)} %reshape.60), channel_id=1, replica_groups=mesh['grp'=2,'kv'=4,'tp'=4] {'kv'}, dimensions={0}, use_global_device_ids=true | all-gather | bytes 40960 | tf_op jit(solution)/shard_map/all_gather | solution.py:91
  77.1 2.6 %convolution_convert_fusion.3 = bf16[16,1024]{1,0:T(8,128)(2,1)} fusion(bf16[16,1024]{1,0:T(8,128)(2,1)S(1)} %reshape.61, bf16[1024,1024]{1,0:T(8,128)(2,1)} %param.27), kind=kOutput, calls=%fused_computation.6 | convolution fusion | flops 33570816 | bytes 2162688 | tf_op jit(solution)/shard_map/dot_general | solution.py:90
  79.6 0.0 reduce-scatter.3.cloned.1.call-update
  79.7 0.0 all-reduce.4.cloned.1.call-start
  79.7 0.0 copy-done.7
  79.7 19.6 %reduce-scatter.3.cloned.1.call-done = bf16[16,256]{1,0:T(8,128)(2,1)} async-done(((bf16[16,1024]{1,0:T(8,128)(2,1)}), bf16[16,256]{1,0:T(8,128)(2,1)}) %reduce-scatter.3.cloned.1.call-update) | async-done | bytes 8208 | tf_op jit(solution)/shard_map/reduce_scatter | solution.py:95
  99.4 0.7 add_convert_fusion.1
  100.1 5.2 %all_gather.17 = bf16[16,1024]{1,0:T(8,128)(2,1)S(1)} all-gather(bf16[16,256]{1,0:T(8,128)(2,1)S(1)} %add_convert_fusion.1), channel_id=1, replica_groups=mesh['grp'=2,'kv'=4,'tp'=4] {'tp'}, dimensions={1}, use_global_device_ids=true | all-gather | bytes 40960 | tf_op jit(solution)/shard_map/all_gather | solution.py:99
  105.2 0.1 fusion.12
  105.4 3.5 %convolution_convert_fusion = bf16[16,2816]{1,0:T(8,128)(2,1)S(1)} fusion(bf16[1024,2816]{1,0:T(8,128)(2,1)} %param.29, bf16[16,1024]{1,0:T(8,128)(2,1)S(1)} %all_gather.17, f32[1024]{0:T(1024)S(1)} %convert_element_type.77), kind=kOutput, calls=%fused_computation | convolution fusion | flops 92368896 | bytes 5894144 | tf_op jit(solution)/shard_map/dot_general | solution.py:104
  108.9 4.1 %convolution_convert_fusion.1 = bf16[16,2816]{1,0:T(8,128)(2,1)} fusion(bf16[1024,2816]{1,0:T(8,128)(2,1)} %param.28, bf16[16,1024]{1,0:T(8,128)(2,1)S(1)} %all_gather.17, f32[1024]{0:T(1024)S(1)} %convert_element_type.77), kind=kOutput, calls=%fused_computation.1 | convolution fusion | flops 92368896 | bytes 5894144 | tf_op jit(solution)/shard_map/dot_general | solution.py:103
  113.0 0.0 all-reduce.4.cloned.1.call-update
  113.0 0.0 reduce-scatter.5.cloned.1.call-start
  113.1 11.8 %psum.23 = f32[16]{0:T(128)S(1)} all-reduce(f32[16]{0:T(128)S(1)} %fusion.12), channel_id=1, replica_groups=mesh['grp'=2,'kv'=4,'tp'=4] {'kv'}, use_global_device_ids=true, to_apply=%region_9.10 | all-reduce | flops 16 | bytes 128 | tf_op jit(solution)/shard_map/psum | solution.py:101
  124.8 14.1 %all-gather = bf16[64,2816]{1,0:T(8,128)(2,1)S(1)} all-gather(bf16[16,2816]{1,0:T(8,128)(2,1)S(1)} %convolution_convert_fusion), channel_id=2, replica_groups=mesh['grp'=2,'kv'=4,'tp'=4] {'kv'}, dimensions={0}, use_global_device_ids=true | all-gather | bytes 450560 | tf_op jit(solution)/shard_map/all_gather | solution.py:108
  139.0 0.1 reduce_sum.62
  139.0 8.6 %all-reduce.4.cloned.1.call-done = bf16[16,2816]{1,0:T(8,128)(2,1)} async-done(((bf16[16,2816]{1,0:T(8,128)(2,1)}), bf16[16,2816]{1,0:T(8,128)(2,1)}) %all-reduce.4.cloned.1.call-update) | async-done | bytes 90128 | tf_op jit(solution)/shard_map/psum | solution.py:107
  147.6 4.2 %convolution_convert_fusion.2 = bf16[16,1024]{1,0:T(8,128)(2,1)} fusion(bf16[2816,1024]{1,0:T(8,128)(2,1)} %param.30, bf16[16,2816]{1,0:T(8,128)(2,1)S(1)} %reduce_sum.62, bf16[16,2816]{1,0:T(8,128)(2,1)} %all-reduce.4.cloned.1.call-done, f32[16]{0:T(128)S(1)} %add_rsqrt_fusion.3), kind=kOutput, calls=%fused_computation.5 | convolution fusion | flops 92741632 | bytes 5980224 | tf_op jit(solution)/shard_map/dot_general | solution.py:115
  151.8 0.0 reduce-scatter.5.cloned.1.call-update
  151.8 19.7 %reduce-scatter.5.cloned.1.call-done = bf16[16,256]{1,0:T(8,128)(2,1)} async-done(((bf16[16,1024]{1,0:T(8,128)(2,1)}), bf16[16,256]{1,0:T(8,128)(2,1)}) %reduce-scatter.5.cloned.1.call-update) | async-done | bytes 8208 | tf_op jit(solution)/shard_map/reduce_scatter | solution.py:116
  171.6 1.3 add_convert_fusion
  (20 shorter events, 0.1 us)
Async XLA Ops:
  7.2 7.4 %copy-start = (bf16[1024,1024]{1,0:T(8,128)(2,1)S(1)}, bf16[1024,1024]{1,0:T(8,128)(2,1)}, u32[]{:S(2)}) copy-start(bf16[1024,1024]{1,0:T(8,128)(2,1)} %param.22) | copy-start | bytes 6291460
  7.2 47.5 %all-reduce.6.cloned.1.call-start = ((), (), s32[]{:S(2)}) async-start(), calls=%async_computation.5 | async-start | bytes 270336
  7.2 7.7 %copy-start.3 = (bf16[1024,1024]{1,0:T(8,128)(2,1)S(1)}, bf16[1024,1024]{1,0:T(8,128)(2,1)}, u32[]{:S(2)}) copy-start(bf16[1024,1024]{1,0:T(8,128)(2,1)} %param.21) | copy-start | bytes 6291460
  14.5 1.6 copy-start.4
  14.9 1.9 %copy-start.5 = (bf16[1024,1024]{1,0:T(8,128)(2,1)S(1)}, bf16[1024,1024]{1,0:T(8,128)(2,1)}, u32[]{:S(2)}) copy-start(bf16[1024,1024]{1,0:T(8,128)(2,1)} %param.19) | copy-start | bytes 6291460
  16.1 1.1 copy-start.9
  16.1 1.1 copy-start.10
  16.1 14.7 %copy-start.11 = (f32[8]{0:T(128)S(1)}, f32[8]{0:T(128)}, u32[]{:S(2)}) copy-start(f32[8]{0:T(128)} %param.25) | copy-start | bytes 100
  16.1 14.8 %copy-start.12 = (u32[32]{0:T(128)S(1)}, u32[32]{0:T(128)}, u32[]{:S(2)}) copy-start(u32[32]{0:T(128)} %constant.48) | copy-start | bytes 388
  18.3 81.1 %reduce-scatter.3.cloned.1.call-start = ((), (), s32[]{:S(2)}) async-start(), calls=%async_computation.2 | async-start | bytes 40960 | tf_op jit(solution)/shard_map/reduce_scatter | solution.py:95
  54.7 5.1 %copy-start.1 = (f32[4,8,128,128]{3,2,1,0:T(8,128)S(1)}, f32[4,8,128,128]{3,2,1,0:T(8,128)}, u32[]{:S(2)}) copy-start(f32[4,8,128,128]{3,2,1,0:T(8,128)} %param.31) | copy-start | bytes 6291460
  60.5 1.3 copy-start.2
  60.5 3.3 %copy-start.8 = (f32[128]{0:T(128)S(1)}, f32[128]{0:T(128)}, u32[]{:S(2)}) copy-start(f32[128]{0:T(128)} %param.26) | copy-start | bytes 1540
  61.8 17.9 %copy-start.7 = (bf16[1024]{0:T(1024)(128)(2,1)S(1)}, bf16[1024]{0:T(1024)(128)(2,1)}, u32[]{:S(2)}) copy-start(bf16[1024]{0:T(1024)(128)(2,1)} %param.18) | copy-start | bytes 6148
  61.8 37.6 %copy-start.6 = (bf16[16,256]{1,0:T(8,128)(2,1)S(1)}, bf16[16,256]{1,0:T(8,128)(2,1)}, u32[]{:S(2)}) copy-start(bf16[16,256]{1,0:T(8,128)(2,1)} %param.16) | copy-start | bytes 24580
  79.7 67.9 %all-reduce.4.cloned.1.call-start = ((), (), s32[]{:S(2)}) async-start(), calls=%async_computation.3 | async-start | bytes 180224 | tf_op jit(solution)/shard_map/psum | solution.py:107
  113.0 58.5 %reduce-scatter.5.cloned.1.call-start = ((), (), s32[]{:S(2)}) async-start(), calls=%async_computation.4 | async-start | bytes 40960 | tf_op jit(solution)/shard_map/reduce_scatter | solution.py:116
Sparse Core Ops, SparseCore 0:
  18.4 36.2 all-reduce.5
  79.8 19.5 reduce-scatter.2
  113.1 34.4 all-reduce.3
  152.0 19.5 reduce-scatter.4
